TPU v7x, 512 devices: a whole 4x8x8 slice. The times are simulated.
512 devices in a mesh: sp: 128 (over z, y, core), tp: 4 (over x).
Axes of the slice: x: 4, y: 8, z: 8, core: 2. Of those that a mesh axis runs over, the one named last changes fastest.
Arguments:
- tokens: bfloat16 [32768, 2048], P(('sp', 'tp')), may hold values from -16 to 16
- w_query: bfloat16 [2048, 1024], P(None, 'tp'), may hold values from -1 to 1
- w_key: bfloat16 [2048, 256], P(None, 'tp'), may hold values from -1 to 1
- w_value: bfloat16 [2048, 256], P(None, 'tp'), may hold values from -0.125 to 0.125
- w_gate: bfloat16 [2048, 16], P(None, 'tp'), may hold values from -0.125 to 0.125
- gate_bias: float32 [16], P('tp'), as said below
- w_output: bfloat16 [1024, 2048], P('tp'), may hold values from -0.1875 to 0.1875
Outputs:
- mixed: bfloat16 [32768, 2048], P(('sp', 'tp'))
Inputs may be any that keep to these rules, and one draw needn't show every extreme that they name: `gate_bias`: each head's forget gate bias is 4 or more; there is no upper bound.
All inputs are finite; a program needn't handle non-finite values.
Results may differ from a plain program's by a relative error of at most 0.012.
The roundings to bfloat16 on the way count: a program that leaves them out, or rounds other values in their place, can miss the bound.
Values may be sent and summed in bfloat16 or wider, within the bound.
A program may use at most 64 MiB of HBM per device.

v0:
```python
import math

import jax
import jax.numpy as jnp
from jax import lax
from jax.sharding import Mesh
from jax.sharding import PartitionSpec as P

HEAD = 64
SP = ("sp_0", "sp_1", "sp_2")
SP_TP = ("sp_0", "sp_1", "sp_2", "tp")


masked_value = -1e30


def copy_for_each(value, axis):
    copies = jnp.broadcast_to(value, (lax.axis_size(axis), *value.shape))
    return lax.all_to_all(copies, axis, split_axis=0, concat_axis=0, tiled=True)


def in_order(pieces, dim):
    lengths = list(pieces.shape[1:])
    lengths[dim] *= pieces.shape[0]
    return jnp.moveaxis(pieces, 0, dim).reshape(lengths)


def collect(value, axis, dim):
    pieces = copy_for_each(value, axis)
    return in_order(pieces, dim)


def all_blocks(value, axes, sequence):
    pieces = value
    for k in sequence:
        pieces = lax.all_gather(pieces, axes[k])
    done = sequence[::-1]
    back = [done.index(k) for k in range(len(axes))]
    pieces = pieces.transpose(*back, *range(len(axes), pieces.ndim))
    return pieces.reshape(-1, *value.shape)


def whole_of(value, axes, sequence, dim):
    return in_order(all_blocks(value, axes, sequence), dim)


def in_blocks(value, dim, count):
    lengths = value.shape
    pieces = value.reshape(*lengths[:dim], count, lengths[dim] // count, *lengths[dim + 1 :])
    return jnp.moveaxis(pieces, dim, 0)


def sum_at_owner(value, axis, dim):
    pieces = in_blocks(value, dim, lax.axis_size(axis))
    arrived = lax.all_to_all(pieces, axis, split_axis=0, concat_axis=0, tiled=True)
    return arrived.astype(jnp.float32).sum(axis=0)


def softmax_update(
    carry_state,
    query_here,
    query_cumul,
    query_position,
    key_here,
    value_here,
    key_cumul,
    key_position,
):
    row_peak, row_mass, row_accum = carry_state
    scores = jnp.einsum(
        "kgtd,skd->kgts", query_here, key_here, preferred_element_type=jnp.float32
    ) * HEAD ** (-0.5)
    scores = scores + query_cumul[:, :, :, None] - key_cumul[:, :, None, :]
    allowed = key_position[None, :] <= query_position[:, None]
    scores = jnp.where(allowed, scores, masked_value)
    new_peak = jnp.maximum(row_peak, jnp.max(scores, axis=3))
    weights = jnp.where(allowed, jnp.exp(scores - new_peak[:, :, :, None]), 0.0)
    rescale = jnp.exp(row_peak - new_peak)
    row_mass = row_mass * rescale + jnp.sum(weights, axis=3)
    row_accum = row_accum * rescale[:, :, :, None] + jnp.einsum(
        "kgts,skd->kgtd",
        weights.astype(jnp.bfloat16),
        value_here,
        preferred_element_type=jnp.float32,
    )
    return (new_peak, row_mass, row_accum)


def shards(tokens, w_query, w_key, w_value, w_gate, gate_bias, w_output):
    sp_count = lax.axis_size(SP)
    sp_rank = lax.axis_index(SP)
    query_cols = w_query.shape[1]
    key_cols = w_key.shape[1]
    heads_here = w_gate.shape[1]
    kv_heads_here = key_cols // HEAD
    group_size = heads_here // kv_heads_here
    joined = jnp.concatenate([w_query, w_key, w_value, w_gate], axis=1)
    projected = jnp.dot(
        collect(tokens, "tp", 0), joined, preferred_element_type=jnp.float32
    ).astype(jnp.bfloat16)
    local_rows = projected.shape[0]
    half_rows = local_rows // 2
    second_block = 2 * sp_rank + 1
    own_gates = jax.nn.log_sigmoid(
        projected[:, query_cols + 2 * key_cols :].astype(jnp.float32) + gate_bias
    )
    totals = jnp.sum(own_gates.reshape(2, half_rows, heads_here), axis=1)
    all_totals = whole_of(totals[None], (("sp_0", "sp_1"), "sp_2"), (0, 1), 0)
    ordered = all_totals.reshape(2 * sp_count, heads_here)
    prefix_sums = jnp.cumsum(ordered, axis=0) - ordered
    queries = (
        projected[:, :query_cols]
        .reshape(2, half_rows, kv_heads_here, group_size, HEAD)
        .transpose(0, 2, 3, 1, 4)
    )
    query_blocks = (2 * sp_rank, second_block)
    query_cumul = []
    query_position = []
    for side_index in range(2):
        base_value = lax.dynamic_index_in_dim(
            prefix_sums, query_blocks[side_index], 0, keepdims=False
        )
        cumul_rows = base_value[None, :] + jnp.cumsum(
            own_gates[side_index * half_rows : (side_index + 1) * half_rows], axis=0
        )
        query_cumul.append(
            cumul_rows.reshape(half_rows, kv_heads_here, group_size).transpose(1, 2, 0)
        )
        query_position.append(
            query_blocks[side_index] * half_rows + jnp.arange(half_rows, dtype=jnp.int32)
        )
    initial = (
        jnp.full((2, kv_heads_here, group_size, half_rows), masked_value, jnp.float32),
        jnp.zeros((2, kv_heads_here, group_size, half_rows), jnp.float32),
        jnp.zeros((2, kv_heads_here, group_size, half_rows, HEAD), jnp.float32),
    )
    gathered = lax.all_gather(projected[:, query_cols:], SP, axis=0, tiled=True)
    row_count = gathered.shape[0]
    piece_blocks = row_count // half_rows
    per_step = math.gcd(piece_blocks, max(1, 1024 // half_rows))
    step_rows = per_step * half_rows
    step_count = row_count // step_rows
    first_row = half_rows * jnp.arange(piece_blocks, dtype=jnp.int32)
    owner_rank = first_row // local_rows
    half_index = first_row % local_rows // half_rows
    block_ids = 2 * owner_rank + half_index
    gate_logs = jax.nn.log_sigmoid(gathered[:, 2 * key_cols :].astype(jnp.float32) + gate_bias)
    gate_logs = gate_logs.reshape(piece_blocks, half_rows, heads_here)
    base_values = jnp.take(prefix_sums, block_ids, axis=0)
    key_cumul_all = (base_values[:, None, :] + jnp.cumsum(gate_logs, axis=1)).reshape(
        row_count, kv_heads_here, group_size
    )
    key_position_all = (
        block_ids[:, None] * half_rows + jnp.arange(half_rows, dtype=jnp.int32)[None, :]
    ).reshape(row_count)
    earliest = jnp.min(block_ids.reshape(step_count, per_step), axis=1)

    def one_step(step_index, inner_state):
        start_row = step_index * step_rows
        block_rows = lax.dynamic_slice_in_dim(gathered, start_row, step_rows, 0)
        key_here = block_rows[:, :key_cols].reshape(step_rows, kv_heads_here, HEAD)
        value_here = block_rows[:, key_cols : 2 * key_cols].reshape(step_rows, kv_heads_here, HEAD)
        key_cumul = lax.dynamic_slice_in_dim(key_cumul_all, start_row, step_rows, 0).transpose(
            1, 2, 0
        )
        key_position = lax.dynamic_slice_in_dim(key_position_all, start_row, step_rows, 0)
        first_id = earliest[step_index]
        results = []
        for side_index in range(2):
            head_state = tuple((member[side_index] for member in inner_state))

            def compute(head_state, side_index=side_index):
                return softmax_update(
                    head_state,
                    queries[side_index],
                    query_cumul[side_index],
                    query_position[side_index],
                    key_here,
                    value_here,
                    key_cumul,
                    key_position,
                )

            head_state = lax.cond(
                first_id <= query_blocks[side_index],
                compute,
                lambda unchanged: unchanged,
                head_state,
            )
            results.append(head_state)
        return tuple((jnp.stack([results[0][member], results[1][member]]) for member in range(3)))

    row_peak, row_mass, row_accum = lax.fori_loop(0, step_count, one_step, initial)
    attended = (row_accum / row_mass[:, :, :, :, None]).astype(jnp.bfloat16)
    attended = attended.transpose(0, 3, 1, 2, 4).reshape(local_rows, heads_here * HEAD)
    mixed = sum_at_owner(
        jnp.dot(attended, w_output, preferred_element_type=jnp.float32).astype(jnp.bfloat16),
        "tp",
        0,
    )
    return mixed.astype(jnp.bfloat16)


def solution(mesh):
    finer = Mesh(mesh.devices.reshape(8, 8, 2, mesh.shape["tp"]), ("sp_0", "sp_1", "sp_2", "tp"))
    placed = (
        P(SP_TP, None),
        P(None, "tp"),
        P(None, "tp"),
        P(None, "tp"),
        P(None, "tp"),
        P("tp"),
        P("tp", None),
    )
    return jax.shard_map(
        shards, mesh=finer, in_specs=placed, out_specs=P(SP_TP, None), check_vma=False
    )
```

profile of v0, /device:TPU:504, one launch (start us, length us, event | category | flops | bytes accessed | tf_op | source)
XLA Modules:
  0.0 388.9 jit_solution(7107253783128811441)
XLA Ops:
  8.7 4.3 %all-to-all-start = ((bf16[4,64,2048]{2,1,0:T(8,128)(2,1)}), bf16[4,64,2048]{2,1,0:T(8,128)(2,1)S(1)}, u32[]{:S(2)}, u32[]{:S(2)}) async-start(bf16[4,64,2048]{2,1,0:T(8,128)(2,1)} %broadcast_in_dim.67), calls=%async_computation | async-start | bytes 2097152 | tf_op jit(solution)/shard_map/all_to_all | solution.py:19
  14.7 13.4 %all-to-all-done = bf16[4,64,2048]{2,1,0:T(8,128)(2,1)S(1)} async-done(((bf16[4,64,2048]{2,1,0:T(8,128)(2,1)}), bf16[4,64,2048]{2,1,0:T(8,128)(2,1)S(1)}, u32[]{:S(2)}, u32[]{:S(2)}) %all-to-all-start) | async-done | bytes 1048608 | tf_op jit(solution)/shard_map/all_to_all | solution.py:19
  28.1 2.5 fusion.47
  31.9 47.2 %all-gather.2 = f32[64,2,4]{2,1,0:T(2,128)S(1)} all-gather(f32[1,2,4]{2,1,0:T(2,128)S(1)} %bitcast.213), channel_id=2, replica_groups=mesh['sp_0'=8,'sp_1'=8,'sp_2'=2,'tp'=4] {'sp_0','sp_1'}, dimensions={0}, use_global_device_ids=true | all-gather | bytes 2080 | tf_op jit(solution)/shard_map/all_gather | solution.py:36
  84.7 35.0 %all-gather.5.cloned.1.call-done = bf16[32768,132]{0,1:T(8,128)(2,1)} async-done(((bf16[256,132]{0,1:T(8,128)(2,1)}), bf16[32768,132]{0,1:T(8,128)(2,1)}) %all-gather.5.cloned.1.call-update) | async-done | bytes 8650768 | tf_op jit(solution)/shard_map/all_gather | solution.py:137
  122.7 238.2 %while.18 = (s32[]{:T(128)}, f32[2,1,4,128]{3,2,1,0:T(4,128)S(1)}, f32[2,1,4,128]{3,2,1,0:T(4,128)S(1)}, f32[2,1,4,128,64]{3,4,2,1,0:T(8,128)S(1)}, s32[32]{0:T(...) while((s32[]{:T(128)}, f32[2,1,4,128]{3,2,1,0:T(4,128)S(1)}, ...), condition=%wide.region_16.17_spmd.clone, body=%wide.region_7.16_spmd.clone.sunk | while | flops 280433920 | bytes 16568903 | solution.py:193
  125.1 2.2 conditional.6
  127.9 2.2 conditional.7
  132.5 2.2 conditional.6
  135.4 2.2 conditional.7
  140.0 2.2 conditional.6
  142.8 2.2 conditional.7
  147.4 2.2 conditional.6
  150.2 2.2 conditional.7
  157.7 2.2 conditional.7
  162.3 2.2 conditional.6
  165.1 2.2 conditional.7
  172.6 2.2 conditional.7
  177.2 2.2 conditional.6
  180.0 2.2 conditional.7
  187.5 2.2 conditional.7
  192.1 2.2 conditional.6
  194.9 2.2 conditional.7
  202.4 2.2 conditional.7
  207.0 2.2 conditional.6
  209.8 2.2 conditional.7
  217.2 2.2 conditional.7
  221.8 2.2 conditional.6
  224.7 2.2 conditional.7
  232.1 2.2 conditional.7
  239.6 2.2 conditional.7
  247.0 2.2 conditional.7
  254.5 2.2 conditional.7
  261.9 2.2 conditional.7
  269.4 2.2 conditional.7
  276.8 2.2 conditional.7
  284.2 2.2 conditional.7
  291.7 2.2 conditional.7
  299.1 2.2 conditional.7
  306.6 2.2 conditional.7
  314.0 2.2 conditional.7
  321.5 2.2 conditional.7
  328.9 2.2 conditional.7
  336.4 2.2 conditional.7
  343.8 2.2 conditional.7
  351.2 2.2 conditional.7
  358.7 2.2 conditional.7
  361.6 19.5 %all_to_all.10 = bf16[4,64,2048]{2,1,0:T(8,128)(2,1)S(1)} all-to-all(bf16[4,64,2048]{2,1,0:T(8,128)(2,1)S(1)} %bitcast.197), channel_id=1, replica_groups=mesh['sp_0'=8,'sp_1'=8,'sp_2'=2,'tp'=4] {'tp'}, dimensions={0} | all-to-all | bytes 2097152 | tf_op jit(solution)/shard_map/all_to_all | solution.py:55
  (891 shorter events, 255.7 us)
Async XLA Ops:
  6.5 354.6 %copy-start = (bf16[256,2048]{1,0:T(8,128)(2,1)S(1)}, bf16[256,2048]{1,0:T(8,128)(2,1)}, u32[]{:S(2)}) copy-start(bf16[256,2048]{1,0:T(8,128)(2,1)} %param.19) | copy-start | bytes 3145732
  6.5 6.5 %copy-start.3 = (bf16[2048,4]{0,1:T(4,128)(2,1)S(1)}, bf16[2048,4]{0,1:T(4,128)(2,1)}, u32[]{:S(2)}) copy-start(bf16[2048,4]{0,1:T(4,128)(2,1)} %param.17) | copy-start | bytes 49156
  6.5 7.6 %copy-start.1 = (bf16[2048,64]{0,1:T(8,128)(2,1)S(1)}, bf16[2048,64]{0,1:T(8,128)(2,1)}, u32[]{:S(2)}) copy-start(bf16[2048,64]{0,1:T(8,128)(2,1)} %param.16) | copy-start | bytes 786436
  6.5 7.8 %copy-start.2 = (bf16[2048,64]{0,1:T(8,128)(2,1)S(1)}, bf16[2048,64]{0,1:T(8,128)(2,1)}, u32[]{:S(2)}) copy-start(bf16[2048,64]{0,1:T(8,128)(2,1)} %param.15) | copy-start | bytes 786436
  8.7 19.4 %all-to-all-start = ((bf16[4,64,2048]{2,1,0:T(8,128)(2,1)}), bf16[4,64,2048]{2,1,0:T(8,128)(2,1)S(1)}, u32[]{:S(2)}, u32[]{:S(2)}) async-start(bf16[4,64,2048]{2,1,0:T(8,128)(2,1)} %broadcast_in_dim.67), calls=%async_computation | async-start | bytes 2097152 | tf_op jit(solution)/shard_map/all_to_all | solution.py:19
  13.0 106.7 %all-gather.5.cloned.1.call-start = ((), (), s32[]{:S(2)}) async-start(), calls=%async_computation.2 | async-start | bytes 8982528 | tf_op jit(solution)/shard_map/all_gather | solution.py:137
  28.1 3.5 copy-start.4
Sparse Core Ops, SparseCore 0:
  31.4 88.1 all-gather.4
where the time goes:
time: 390 us; the launch traced here: 389 us
  matrix products  91.4 us (23%)
  blocking collectives  68.7 us (18%)
  local copies, waits for them, and re-layouts  59.3 us (15%)
  other arithmetic  55.4 us (14%)
  waiting for transfers between devices  48.4 us (12%)
  loops' own time  47.7 us (12%)
  between operations  13.7 us (4%)
  starting transfers between devices  4.29 us (1%)
    all_gather x2, blocking collectives, all_blocks(): pieces = lax.all_gather(pieces, axes[k])  49.1 us
    dot_general x64, matrix products, softmax_update(): jnp.einsum('kgtd,skd->kgts', query_here, key_here, preferred_element_type...  48.9 us
    another operation x1, loops' own time, shards(): lax.fori_loop(0, step_count, one_step, initial)  45.3 us
    dot_general x64, matrix products, softmax_update(): jnp.einsum('kgts,skd->kgtd', weights.astype(jnp.bfloat16), value_here, pr...  39.5 us
    reduce_sum x64, other arithmetic, softmax_update(): row_mass = row_mass * rescale + jnp.sum(weights, axis=3)  37.9 us
    all_gather x1, waiting for transfers between devices, shards(): gathered = lax.all_gather(projected[:, query_cols:], SP, axis=0, tiled=True)  35 us
    reshape x32, local copies, waits for them, and re-layouts, one_step(): block_rows[:, key_cols:2 * key_cols].reshape(step_rows, kv_heads_here, HEAD)  31.8 us
    all_to_all x1, blocking collectives, sum_at_owner(): lax.all_to_all(pieces, axis, split_axis=0, concat_axis=0, tiled=True)  19.5 us
  transfers between devices with their start and end apart: 2, of which 2 were waited for; matrix products, arithmetic and copies ran while one was open for 1% of the time, Pallas kernels for 0%

commit v1 on v0

v1 whole, which is shorter than its diff:
```python
import functools

import jax
import jax.numpy as jnp
from jax import lax
from jax.experimental import pallas as pl
from jax.experimental.pallas import tpu as pltpu
from jax.sharding import Mesh
from jax.sharding import PartitionSpec as P

HEAD = 64
BLOCK = 256
HALF = 128
ROWS = 144
LOG2E = 1.4426950408889634
LOW = -1e30
AXES = ("sp_0", "sp_1", "sp_2", "tp")
SP_TP = AXES
MESH = pl.DeviceIdType.MESH
f32 = jnp.float32
bf16 = jnp.bfloat16


def place():
    return tuple(lax.axis_index(a) for a in AXES)


def greet(peers):
    barrier = pltpu.get_barrier_semaphore()
    for peer in peers:
        pl.semaphore_signal(barrier, inc=1, device_id=peer, device_id_type=MESH)
    pl.semaphore_wait(barrier, len(peers))


def remote(src, dst, send, recv, device):
    return pltpu.make_async_remote_copy(
        src_ref=src, dst_ref=dst, send_sem=send, recv_sem=recv,
        device_id=device, device_id_type=MESH,
    )


def three(x):
    a = x.astype(bf16).astype(f32)
    r = x - a
    b = r.astype(bf16).astype(f32)
    return a, b, r - b


def iota(shape, dim):
    return lax.broadcasted_iota(jnp.int32, shape, dim)


def project_kernel(
    tokens, w_q, w_k, w_v, w_g, bias, kv_out, q_out,
    x_all, wq_v, wk_v, wv_v, wg_v, send, recv, local,
):
    z, y, c, x = place()
    n = 4
    peers = [(z, y, c, lax.rem(x + k, n)) for k in range(1, n)]
    loads = [
        pltpu.make_async_copy(src, dst, local.at[i])
        for i, (src, dst) in enumerate(((w_q, wq_v), (w_k, wk_v), (w_v, wv_v), (w_g, wg_v)))
    ]
    for load in loads:
        load.start()
    greet(peers)
    copies = [
        remote(tokens, x_all.at[x], send.at[k], recv.at[k], peers[k]) for k in (0, 2, 1)
    ]
    for copy in copies:
        copy.start()
    x_all[x] = tokens[...]
    for load in loads:
        load.wait()
    for copy in copies:
        copy.wait()
    rows = x_all[...].reshape(BLOCK, x_all.shape[2])

    def dot(a, b):
        return jnp.dot(a, b, preferred_element_type=f32)

    keys = dot(rows, wk_v[...]).astype(bf16).astype(f32)
    values = dot(rows, wv_v[...]).astype(bf16).astype(f32)
    kv = jnp.concatenate([keys, values], axis=1).T
    kv_out[0:HALF, :] = kv.astype(bf16)

    gates = dot(rows, wg_v[...]).astype(bf16).astype(f32) + bias[...]
    heads = gates.shape[1]
    gates = jnp.concatenate([gates, jnp.zeros((BLOCK, 128 - heads), f32)], axis=1).T[0:8]
    small = jnp.exp(-jnp.abs(gates))
    series = small * (1.0 - small * (0.5 - small * (1 / 3 - small * (0.25 - small * 0.2))))
    logs = jnp.minimum(gates, 0.0) - jnp.where(small < 0.02, series, jnp.log(1.0 + small))
    tri = (iota((BLOCK, BLOCK), 0) <= iota((BLOCK, BLOCK), 1)).astype(f32).astype(bf16)
    pieces = jnp.concatenate([*three(logs), jnp.zeros((8, BLOCK), f32)], axis=0)
    sums = dot(pieces.astype(bf16), tri)
    decay = (sums[0:8] + sums[8:16] + sums[16:24]) * (-LOG2E)
    hi, mid, lo = three(decay)
    row = iota((8, BLOCK), 0)
    first = jnp.where(row < 4, hi, pltpu.roll(mid, 4, 0))
    second = jnp.where(row < 4, lo, 0.0)
    kv_out[HALF:ROWS, :] = jnp.concatenate([first, second], axis=0).astype(bf16)

    queries = dot(rows, wq_v[...]).astype(bf16).astype(f32) * (LOG2E * HEAD**-0.5)
    top = queries.astype(bf16).astype(f32)
    rest = queries - top
    for h in range(4):
        cols = slice(h * HEAD, (h + 1) * HEAD)
        both = jnp.concatenate([top[:, cols], rest[:, cols]], axis=1).astype(bf16)
        for part in range(2):
            q_out[part, h * HALF : (h + 1) * HALF, :] = both[part * HALF : (part + 1) * HALF]


def project(tokens, w_q, w_k, w_v, w_g, bias):
    d = tokens.shape[1]
    vmem = pl.BlockSpec(memory_space=pltpu.VMEM)
    anyspace = pl.BlockSpec(memory_space=pl.ANY)
    return pl.pallas_call(
        project_kernel,
        name="project",
        out_shape=(
            jax.ShapeDtypeStruct((ROWS, BLOCK), bf16),
            jax.ShapeDtypeStruct((2, 4 * HALF, 128), bf16),
        ),
        in_specs=[vmem, anyspace, anyspace, anyspace, anyspace, vmem],
        out_specs=(vmem, vmem),
        scratch_shapes=[
            pltpu.VMEM((4, tokens.shape[0], d), bf16),
            pltpu.VMEM(w_q.shape, bf16),
            pltpu.VMEM(w_k.shape, bf16),
            pltpu.VMEM(w_v.shape, bf16),
            pltpu.VMEM(w_g.shape, bf16),
            pltpu.SemaphoreType.DMA((3,)),
            pltpu.SemaphoreType.DMA((3,)),
            pltpu.SemaphoreType.DMA((4,)),
        ],
        compiler_params=pltpu.CompilerParams(
            collective_id=0, has_side_effects=True, vmem_limit_bytes=24 * 2**20
        ),
    )(tokens, w_q, w_k, w_v, w_g, bias)


def block_rank(core, a, b):
    zz = a * (1 - core) + b * core
    yy = b * (1 - core) + a * core
    return zz * 16 + yy * 2 + core


def attend_kernel(
    own_kv, queries, w_own, att_out, w_all,
    buf, q_aug, q_in, peak, accum, table,
    local, one_send, one_recv, right_send, right_recv, left_send, left_recv,
    sib_send, sib_recv, q_send, q_recv, w_send, w_recv, ws_send, ws_recv,
):
    z, y, c, x = place()
    a0 = z * (1 - c) + y * c
    b0 = y * (1 - c) + z * c
    rank = z * 16 + y * 2 + c
    ring = [
        (lax.rem(z + k * c, 8), lax.rem(y + k * (1 - c), 8), c, x) for k in range(1, 8)
    ]
    right = (lax.rem(z + (1 - c), 8), lax.rem(y + c, 8), c, x)
    left = (lax.rem(z + 7 * (1 - c), 8), lax.rem(y + 7 * c, 8), c, x)
    sibling = (z, y, 1 - c, x)
    mirror = (7 - z, 7 - y, 1 - c, x)
    across = [(z, y, c, lax.rem(x + k, 4)) for k in range(1, 4)]

    own_load = pltpu.make_async_copy(own_kv, buf.at[c, a0, b0], local.at[0])
    q_load = pltpu.make_async_copy(queries.at[0], q_aug.at[0, :, pl.ds(0, 128)], local.at[1])
    own_load.start()
    q_load.start()
    greet([*ring, right, left, sibling, mirror, *across])
    own_load.wait()

    ones = [
        remote(buf.at[c, a0, b0], buf.at[c, a0, b0], one_send.at[k - 1], one_recv.at[k - 1], ring[k - 1])
        for k in range(1, 8)
    ]
    for k in (1, 7, 2, 6, 3, 5, 4):
        ones[k - 1].start()
    q_copy = remote(queries.at[1], q_aug.at[1, :, pl.ds(0, 128)], q_send, q_recv, mirror)
    q_copy.start()
    half_rows = pl.ds(pl.multiple_of(c * 128, 128), 128)
    w_copies = [
        remote(w_own.at[half_rows], w_all.at[x, half_rows], w_send.at[k], w_recv.at[k], across[k])
        for k in range(3)
    ]
    for k in (0, 2, 1):
        w_copies[k].start()

    selector = (
        (iota((4 * HALF, 128), 1) < 12)
        & (lax.rem(iota((4 * HALF, 128), 1), 4) == iota((4 * HALF, 128), 0) // HALF)
    ).astype(f32).astype(bf16)
    q_aug[0, :, 128:256] = selector
    q_aug[1, :, 128:256] = selector
    peak[...] = jnp.full(peak.shape, LOW, f32)
    accum[...] = jnp.zeros(accum.shape, f32)

    for copy in ones:
        copy.wait()

    def chunk(core, a, ch):
        return buf.at[core, a, pl.ds(ch * 4, 4)]

    def to_right(d, ch, i):
        ref = chunk(c, lax.rem(a0 - d + 8, 8), ch)
        return remote(ref, ref, right_send.at[i], right_recv.at[i], right)

    def to_left(d, ch, i):
        ref = chunk(c, lax.rem(a0 + d, 8), ch)
        return remote(ref, ref, left_send.at[i], left_recv.at[i], left)

    def to_sibling(a, ch, i):
        ref = chunk(c, a, ch)
        return remote(ref, ref, sib_send.at[i], sib_recv.at[i], sibling)

    for ch in range(2):
        to_right(0, ch, ch).start()
        to_left(0, ch, ch).start()
    for ch in range(2):
        to_sibling(a0, ch, ch).start()

    def hop(i, carry):
        d = i // 2 + 1
        ch_r = lax.rem(i, 2)
        ch_l = lax.rem(i, 2) + i // 6
        a_r = lax.rem(a0 - d + 8, 8)
        a_l = lax.rem(a0 + d, 8)
        got = chunk(c, a_r, ch_r)
        remote(got, got, right_send.at[i], right_recv.at[i], right).wait_recv()

        @pl.when(i <= 4)
        def _():
            to_right(d, ch_r, i + 2).start()

        to_sibling(a_r, ch_r, 2 + 2 * i).start()
        got = chunk(c, a_l, ch_l)
        remote(got, got, left_send.at[i], left_recv.at[i], left).wait_recv()

        @pl.when(i <= 3)
        def _():
            to_left(d, ch_l, i + 2).start()

        @pl.when(i == 5)
        def _():
            to_left(d, ch_l, 6).start()

        to_sibling(a_l, ch_l, 3 + 2 * i).start()
        return carry

    lax.fori_loop(0, 7, hop, 0)

    def drain(i, carry):
        ref = chunk(c, a0, 0)
        to_sibling(a0, 0, i).wait_recv()
        to_sibling(a0, 0, i).wait_send()
        return carry

    lax.fori_loop(0, 16, drain, 0)

    def drain_ring(i, carry):
        to_right(0, 0, i).wait_send()
        to_left(0, 0, i).wait_send()
        return carry

    lax.fori_loop(0, 7, drain_ring, 0)
    q_copy.wait()
    q_load.wait()

    def total(r, acc):
        core = lax.rem(r, 2)
        yy = lax.rem(r // 2, 8)
        zz = r // 16
        a = zz * (1 - core) + yy * core
        b = yy * (1 - core) + zz * core
        last = buf[core, a, b, HALF:ROWS, 128:256].astype(f32)[:, 127:128]
        return jnp.where(iota((16, 128), 1) == r, last, acc)

    totals = lax.fori_loop(0, 128, total, jnp.zeros((16, 128), f32))
    before = (iota((128, 128), 0) < iota((128, 128), 1)).astype(f32).astype(bf16)
    offset = jnp.dot(totals.astype(bf16), before, preferred_element_type=f32)
    offset = offset[0:8] + pltpu.roll(offset[0:8], 4, 0) + offset[8:16]
    for h in range(4):
        table[h] = jnp.broadcast_to(offset[h : h + 1], (128, 128)).T

    ones_rows = jnp.ones((16, 2 * BLOCK), bf16)
    zero_rows = jnp.zeros((112, 2 * BLOCK), bf16)

    def pair(part, core, a, j, masked):
        my_rank = rank * (1 - part) + (127 - rank) * part
        b = 2 * j

        def both(lo, hi):
            return jnp.concatenate(
                [buf[core, a, b, lo:hi, :], buf[core, a, b + 1, lo:hi, :]], axis=1
            )

        keys = both(0, HEAD)
        right_side = jnp.concatenate([keys, keys, both(HALF, ROWS), zero_rows], axis=0)
        scores = jnp.dot(q_aug[part], right_side, preferred_element_type=f32)
        sides = []
        peaks = [peak[part]]
        for u in range(2):
            their = block_rank(core, a, b + u)
            shift = jnp.concatenate(
                [
                    jnp.broadcast_to(table[h, pl.ds(their, 1), :], (HALF, 128))
                    for h in range(4)
                ],
                axis=0,
            )
            s = scores[:, u * BLOCK : (u + 1) * BLOCK]
            allowed = None
            if masked:
                q_at = my_rank * BLOCK + part * HALF + lax.rem(iota(s.shape, 0), HALF)
                k_at = their * BLOCK + iota(s.shape, 1)
                allowed = k_at <= q_at
                s = jnp.where(allowed, s, LOW)
            peaks.append(jnp.max(s, axis=1, keepdims=True) + shift)
            sides.append((s, shift, allowed))
        new_peak = jnp.maximum(jnp.maximum(peaks[0], peaks[1]), peaks[2])
        weights = []
        for s, shift, allowed in sides:
            base = new_peak - shift
            w = jnp.exp2(s - jnp.concatenate([base, base], axis=1))
            if masked:
                w = jnp.where(allowed, w, 0.0)
            weights.append(w.astype(bf16))
        values = jnp.concatenate([both(HEAD, HALF), ones_rows, zero_rows[0:48]], axis=0)
        gained = lax.dot_general(
            jnp.concatenate(weights, axis=1), values, (((1,), (1,)), ((), ())),
            preferred_element_type=f32,
        )
        accum[part] = accum[part] * jnp.exp2(peaks[0] - new_peak) + gained
        peak[part] = new_peak

    def visit(t, carry):
        part = t // 64
        u = lax.rem(t, 64)
        core = u // 32
        a = lax.rem(u // 4, 8)
        j = lax.rem(u, 4)
        my_rank = rank * (1 - part) + (127 - rank) * part
        low = block_rank(core, a, 2 * j)
        high = block_rank(core, a, 2 * j + 1)

        @pl.when(high < my_rank)
        def _():
            pair(part, core, a, j, False)

        @pl.when((low <= my_rank) & (high >= my_rank))
        def _():
            pair(part, core, a, j, True)

        return carry

    lax.fori_loop(0, 128, visit, 0)

    for part in range(2):
        total_of = accum[part]
        out = total_of[:, 0:HEAD] / total_of[:, HEAD : HEAD + 1]
        for h in range(4):
            att_out[part, :, h * HEAD : (h + 1) * HEAD] = out[h * HALF : (h + 1) * HALF].astype(bf16)

    for k in range(3):
        w_copies[k].wait()
    shared = []
    for k in range(3):
        who = lax.rem(x + 3 - k, 4)
        ref = w_all.at[who, half_rows]
        shared.append(remote(ref, ref, ws_send.at[k], ws_recv.at[k], sibling))
        shared[-1].start()
    for copy in shared:
        copy.wait()


def attend(own_kv, queries, w_output):
    vmem = pl.BlockSpec(memory_space=pltpu.VMEM)
    anyspace = pl.BlockSpec(memory_space=pl.ANY)
    dma = pltpu.SemaphoreType.DMA
    return pl.pallas_call(
        attend_kernel,
        name="attend",
        out_shape=(
            jax.ShapeDtypeStruct((2, HALF, 4 * HEAD), bf16),
            jax.ShapeDtypeStruct((4, *w_output.shape), bf16),
        ),
        in_specs=[anyspace, anyspace, anyspace],
        out_specs=(vmem, anyspace),
        scratch_shapes=[
            pltpu.VMEM((2, 8, 8, ROWS, BLOCK), bf16),
            pltpu.VMEM((2, 4 * HALF, 256), bf16),
            pltpu.VMEM((8, 128), bf16),
            pltpu.VMEM((2, 4 * HALF, 128), f32),
            pltpu.VMEM((2, 4 * HALF, 128), f32),
            pltpu.VMEM((4, 128, 128), f32),
            dma((2,)),
            dma((7,)), dma((7,)),
            dma((7,)), dma((7,)),
            dma((7,)), dma((7,)),
            dma((16,)), dma((16,)),
            dma, dma,
            dma((3,)), dma((3,)),
            dma((3,)), dma((3,)),
        ],
        compiler_params=pltpu.CompilerParams(
            collective_id=1, has_side_effects=True, vmem_limit_bytes=48 * 2**20
        ),
    )(own_kv, queries, w_output)


def output_kernel(att, w_own, w_all, out, heads, w_v, send, recv, local):
    z, y, c, x = place()
    n = 4
    here = [(z, y, c, lax.rem(x + k, n)) for k in range(1, n)]
    there = [(7 - z, 7 - y, 1 - c, g) for g in range(n)]
    loads = [pltpu.make_async_copy(w_own, w_v.at[x], local.at[0])]
    for k in range(1, n):
        g = lax.rem(x + k, n)
        loads.append(pltpu.make_async_copy(w_all.at[g], w_v.at[g], local.at[k]))
    for load in loads:
        load.start()
    greet([*here, *there])

    def to(owner):
        part = owner // 2
        device = there[owner] if part else (z, y, c, owner)
        src = att.at[part, pl.ds((owner % 2) * 64, 64), :]
        return remote(src, heads.at[x], send.at[owner], recv.at[x], device)

    for owner in range(n):
        if owner < 2:

            @pl.when(x != owner)
            def _(owner=owner):
                to(owner).start()

            @pl.when(x == owner)
            def _(owner=owner):
                heads[owner] = att[0, owner * 64 : (owner + 1) * 64, :]
        else:
            to(owner).start()

    for load in loads:
        load.wait()
    for g in range(n):
        arrives = (x >= 2) | (x != g)

        @pl.when(arrives)
        def _(g=g):
            src = att.at[0, pl.ds(0, 64), :]
            remote(src, heads.at[g], send.at[0], recv.at[g], there[0]).wait_recv()

    for col in range(0, out.shape[1], 512):
        total = None
        for g in range(n):
            part = jnp.dot(heads[g], w_v[g, :, col : col + 512], preferred_element_type=f32)
            part = part.astype(bf16).astype(f32)
            total = part if total is None else total + part
        out[:, col : col + 512] = total.astype(bf16)

    for owner in range(n):
        if owner < 2:

            @pl.when(x != owner)
            def _(owner=owner):
                to(owner).wait_send()
        else:
            to(owner).wait_send()


def output(att, w_own, w_all):
    d = w_own.shape[1]
    vmem = pl.BlockSpec(memory_space=pltpu.VMEM)
    anyspace = pl.BlockSpec(memory_space=pl.ANY)
    dma = pltpu.SemaphoreType.DMA
    return pl.pallas_call(
        output_kernel,
        name="output",
        out_shape=jax.ShapeDtypeStruct((64, d), bf16),
        in_specs=[vmem, anyspace, anyspace],
        out_specs=vmem,
        scratch_shapes=[
            pltpu.VMEM((4, 64, 4 * HEAD), bf16),
            pltpu.VMEM(w_all.shape, bf16),
            dma((4,)), dma((4,)), dma((4,)),
        ],
        compiler_params=pltpu.CompilerParams(
            collective_id=2, has_side_effects=True, vmem_limit_bytes=24 * 2**20
        ),
    )(att, w_own, w_all)


def shards(tokens, w_query, w_key, w_value, w_gate, gate_bias, w_output):
    own_kv, queries = project(
        tokens, w_query, w_key, w_value, w_gate, gate_bias.reshape(1, -1)
    )
    att, w_all = attend(own_kv, queries, w_output)
    return output(att, w_output, w_all)


def solution(mesh):
    finer = Mesh(mesh.devices.reshape(8, 8, 2, mesh.shape["tp"]), AXES)
    placed = (
        P(SP_TP, None),
        P(None, "tp"),
        P(None, "tp"),
        P(None, "tp"),
        P(None, "tp"),
        P("tp"),
        P("tp", None),
    )
    return jax.shard_map(
        shards, mesh=finer, in_specs=placed, out_specs=P(SP_TP, None), check_vma=False
    )
```

time: 390 us -> 152 us (0.39)
  the two profiles are of different devices: /device:TPU:504 before, /device:TPU:79 now
where the time goes in v1:
time: 152 us; the launch traced here: 151 us
  Pallas kernels  144 us (95%)
  local copies, waits for them, and re-layouts  7.1 us (5%)
    pallas_call x1, Pallas kernels, attend(): pl.pallas_call(attend_kernel, name='attend', out_shape=(jax.ShapeDtypeStr...  112 us
    pallas_call x1, Pallas kernels, project(): pl.pallas_call(project_kernel, name='project', out_shape=(jax.ShapeDtypeS...  16.7 us
    pallas_call x1, Pallas kernels, output(): pl.pallas_call(output_kernel, name='output', out_shape=jax.ShapeDtypeStru...  15.5 us
    unnamed x12, local copies, waits for them, and re-layouts  7.1 us

profile of v1, /device:TPU:79, one launch (start us, length us, event | category | flops | bytes accessed | tf_op | source)
XLA Modules:
  0.0 151.4 jit_solution(7039797375562837251)
XLA Ops:
  0.0 0.0 copy-start
  0.0 1.3 copy.8.w_k
  1.3 1.2 copy.9.w_v
  2.6 1.0 copy.10.w_g
  3.6 0.0 copy-start.1
  3.6 1.2 copy-done.1
  4.8 0.0 copy-start.2
  4.8 0.9 copy-done.2
  5.8 0.0 copy-start.3
  5.8 0.7 copy-done.3
  6.4 16.7 %project.1 = (bf16[144,256]{1,0:T(8,128)(2,1)S(1)}, bf16[2,512,128]{2,1,0:T(8,128)(2,1)S(1)}) custom-call(bf16[64,2048]{1,0:T(8,128)(2,1)S(1)} %copy-done.2, bf16[2048,256]{1,0:T(8,128)(2,1)S(1)} %copy-done.1, bf16[2048,64]{1,0:T(8,128)(2,1)S(1)} %copy.8.w_k, bf16[2048,64]{1,0:T(8,128)(2,1)S(1)} %copy.9.w_v, bf16[2048,4]{1,0:T(8,128)(2,1)S(1)} %copy.10.w_g, ...), custom_call_target="tpu_custom_call" | custom-call | tf_op jit(solution)/shard_map/project/pallas_call | solution.py:117
  23.2 0.0 copy-done
  23.2 112.1 %attend.1 = (bf16[2,128,256]{2,1,0:T(8,128)(2,1)S(1)}, bf16[4,256,2048]{2,1,0:T(8,128)(2,1)S(1)}) custom-call(bf16[144,256]{1,0:T(8,128)(2,1)S(1)} %get-tuple-element.9.own_kv, bf16[2,512,128]{2,1,0:T(8,128)(2,1)S(1)} %get-tuple-element.10.queries, bf16[256,2048]{1,0:T(8,128)(2,1)S(1)} %copy-done), custom_call_target="tpu_custom_call" | custom-call | tf_op jit(solution)/shard_map/attend/pallas_call | solution.py:381
  135.2 15.5 %output.1 = bf16[64,2048]{1,0:T(8,128)(2,1)S(1)} custom-call(bf16[2,128,256]{2,1,0:T(8,128)(2,1)S(1)} %get-tuple-element.11.att, bf16[256,2048]{1,0:T(8,128)(2,1)S(1)} %copy-done, bf16[4,256,2048]{2,1,0:T(8,128)(2,1)S(1)} %get-tuple-element.12.w_all), custom_call_target="tpu_custom_call" | custom-call | tf_op jit(solution)/shard_map/output/pallas_call | solution.py:477
  150.7 0.7 copy.12
Async XLA Ops:
  0.0 23.2 %copy-start = (bf16[256,2048]{1,0:T(8,128)(2,1)S(1)}, bf16[256,2048]{1,0:T(8,128)(2,1)}, u32[]{:S(2)}) copy-start(bf16[256,2048]{1,0:T(8,128)(2,1)} %w_own.3) | copy-start | bytes 3145732
  3.6 1.2 copy-start.1
  4.8 0.9 copy-start.2
  5.8 0.7 copy-start.3

commit v2 on v0

v2 whole, which is shorter than its diff:
```python
import jax
import jax.numpy as jnp
from jax import lax
from jax.experimental import pallas as pl
from jax.experimental.pallas import tpu as pltpu
from jax.sharding import Mesh
from jax.sharding import PartitionSpec as P

HEAD = 64
BLOCK = 256
HALF = 128
ROWS = 144
LOG2E = 1.4426950408889634
LOW = -1e30
AXES = ("sp_0", "sp_1", "sp_2", "tp")
SP_TP = AXES
MESH = pl.DeviceIdType.MESH
f32 = jnp.float32
bf16 = jnp.bfloat16


def remote(src, dst, send, recv, device):
    return pltpu.make_async_remote_copy(
        src_ref=src, dst_ref=dst, send_sem=send, recv_sem=recv,
        device_id=device, device_id_type=MESH,
    )


def three(x):
    a = x.astype(bf16).astype(f32)
    r = x - a
    b = r.astype(bf16).astype(f32)
    return a, b, r - b


def iota(shape, dim):
    return lax.broadcasted_iota(jnp.int32, shape, dim)


def dot(a, b):
    return jnp.dot(a, b, preferred_element_type=f32)


def dot_t(a, b):
    return lax.dot_general(a, b, (((1,), (1,)), ((), ())), preferred_element_type=f32)


def block_rank(core, a, b):
    zz = a * (1 - core) + b * core
    yy = b * (1 - core) + a * core
    return zz * 16 + yy * 2 + core


def layer_kernel(
    tokens, w_q, w_kt, w_vt, w_gt, bias, w_o, out,
    x_all, wq_v, wk_v, wv_v, wg_v, bias_v, w_all, buf, sums_of, q_aug, q_far, peak, accum, table,
    att, heads,
    local, tok_send, tok_recv, one_send, one_recv, ta_send, ta_recv, tb_send, tb_recv,
    ts_send, ts_recv, right_send, right_recv, left_send, left_recv, sib_send, sib_recv,
    q_send, q_recv, w_send, w_recv, ws_send, ws_recv, att_send, att_recv,
):
    z, y, c, x = (lax.axis_index(a) for a in AXES)
    a0 = z * (1 - c) + y * c
    b0 = y * (1 - c) + z * c
    rank = z * 16 + y * 2 + c
    across = [(z, y, c, lax.rem(x + k, 4)) for k in range(1, 4)]
    ring = [(lax.rem(z + k * c, 8), lax.rem(y + k * (1 - c), 8), c, x) for k in range(1, 8)]
    cross = [(lax.rem(z + k * (1 - c), 8), lax.rem(y + k * c, 8), c, x) for k in range(1, 8)]
    right, left = cross[0], cross[6]
    sibling = (z, y, 1 - c, x)
    mirrors = [(7 - z, 7 - y, 1 - c, g) for g in range(4)]
    mirror = (7 - z, 7 - y, 1 - c, x)

    loads = [
        pltpu.make_async_copy(src, dst, local.at[i])
        for i, (src, dst) in enumerate((
            (tokens, x_all.at[x]), (w_kt, wk_v), (w_vt, wv_v), (w_gt, wg_v), (bias, bias_v),
            (w_q, wq_v), (w_o, w_all.at[x]),
        ))
    ]
    for load in loads:
        load.start()
    barrier = pltpu.get_barrier_semaphore()
    peers = [*mirrors, *cross, *ring, *across, sibling]
    for peer in peers:
        pl.semaphore_signal(barrier, inc=1, device_id=peer, device_id_type=MESH)
    loads[0].wait()
    pl.semaphore_wait(barrier, len(peers))

    toks = [remote(x_all.at[x], x_all.at[x], tok_send.at[k], tok_recv.at[k], across[k]) for k in range(3)]
    for k in (0, 2, 1):
        toks[k].start()

    lanes = iota((4 * HALF, 128), 1)
    selector = (
        (lanes < 12) & (lax.rem(lanes, 4) == iota((4 * HALF, 128), 0) // HALF)
    ).astype(f32).astype(bf16)
    q_aug[0, :, 128:256] = selector
    q_aug[1, :, 128:256] = selector
    peak[...] = jnp.full(peak.shape, LOW, f32)
    accum[...] = jnp.zeros(accum.shape, f32)
    for load in loads[1:]:
        load.wait()
    for k in range(3):
        toks[k].wait_recv()

    rows = x_all[...].reshape(BLOCK, x_all.shape[2])
    gates = dot_t(wg_v[...], rows).astype(bf16).astype(f32)
    spread = jnp.broadcast_to(bias_v[...], (4, 4))
    column = jnp.sum(jnp.where(iota((4, 4), 0) == iota((4, 4), 1), spread, 0.0), axis=1, keepdims=True)
    gates = jnp.concatenate([gates + column, jnp.zeros((4, BLOCK), f32)], axis=0)
    buf[c, a0, b0, 0:HEAD, :] = dot_t(wk_v[...], rows).astype(bf16)
    buf[c, a0, b0, HEAD:HALF, :] = dot_t(wv_v[...], rows).astype(bf16)
    small = jnp.exp(-jnp.abs(gates))
    series = small * (1.0 - small * (0.5 - small * (1 / 3 - small * (0.25 - small * 0.2))))
    logs = jnp.minimum(gates, 0.0) - jnp.where(small < 0.02, series, jnp.log(1.0 + small))
    tri = (iota((BLOCK, BLOCK), 0) <= iota((BLOCK, BLOCK), 1)).astype(f32).astype(bf16)
    pieces = jnp.concatenate([*three(logs), jnp.zeros((8, BLOCK), f32)], axis=0)
    sums = dot(pieces.astype(bf16), tri)
    decay = (sums[0:8] + sums[8:16] + sums[16:24]) * (-LOG2E)
    hi, mid, lo = three(decay)
    row = iota((8, BLOCK), 0)
    first = jnp.where(row < 4, hi, pltpu.roll(mid, 4, 0))
    second = jnp.where(row < 4, lo, 0.0)
    last = jnp.broadcast_to(decay[:, BLOCK - 1 : BLOCK], (8, 128))
    ends = jnp.where((iota((8, 128), 0) == iota((8, 128), 1)) & (iota((8, 128), 0) < 4), last, 0.0)
    sums_of[c, a0, b0] = jnp.sum(ends, axis=0, keepdims=True)
    buf[c, a0, b0, HALF:ROWS, :] = jnp.concatenate([first, second], axis=0).astype(bf16)

    own_sum = sums_of.at[c, a0, b0]
    tas = [remote(own_sum, own_sum, ta_send.at[k], ta_recv.at[k], ring[k]) for k in range(7)]
    for k in range(7):
        tas[k].start()
    own = buf.at[c, a0, b0]
    ones = [remote(own, own, one_send.at[k], one_recv.at[k], ring[k]) for k in range(7)]
    for k in (0, 6, 1, 5, 2, 4, 3):
        ones[k].start()

    queries = dot(rows, wq_v[...]).astype(bf16).astype(f32) * (LOG2E * HEAD**-0.5)
    top = queries.astype(bf16).astype(f32)
    rest = queries - top
    for h in range(4):
        cols = slice(h * HEAD, (h + 1) * HEAD)
        both = jnp.concatenate([top[:, cols], rest[:, cols]], axis=1).astype(bf16)
        q_aug[0, h * HALF : (h + 1) * HALF, 0:128] = both[0:HALF]
        q_far[h * HALF : (h + 1) * HALF, :] = both[HALF:]
    for k in range(3):
        toks[k].wait_send()
    q_copy = remote(q_far, q_aug.at[1, :, pl.ds(0, 128)], q_send, q_recv, mirror)
    q_copy.start()
    half_rows = pl.ds(pl.multiple_of(c * 128, 128), 128)
    own_half = w_all.at[x, half_rows]
    w_copies = [remote(own_half, own_half, w_send.at[k], w_recv.at[k], across[k]) for k in range(3)]
    for k in (0, 2, 1):
        w_copies[k].start()

    for k in range(7):
        tas[k].wait()
    eight = sums_of.at[c, a0]
    tbs = [remote(eight, eight, tb_send.at[k], tb_recv.at[k], cross[k]) for k in range(7)]
    for k in range(7):
        tbs[k].start()

    def chunk(core, a, ch):
        return buf.at[core, a, pl.ds(ch * 4, 4)]

    def to_right(d, ch, i):
        ref = chunk(c, lax.rem(a0 - d + 8, 8), ch)
        return remote(ref, ref, right_send.at[i], right_recv.at[i], right)

    def to_left(d, ch, i):
        ref = chunk(c, lax.rem(a0 + d, 8), ch)
        return remote(ref, ref, left_send.at[i], left_recv.at[i], left)

    def to_sibling(a, ch, i):
        ref = chunk(c, a, ch)
        return remote(ref, ref, sib_send.at[i], sib_recv.at[i], sibling)

    for k in range(7):
        ones[k].wait()
    for ch in range(2):
        to_right(0, ch, ch).start()
        to_left(0, ch, ch).start()
    for ch in range(2):
        to_sibling(a0, ch, ch).start()

    for k in range(7):
        tbs[k].wait()
    core_sums = sums_of.at[c]
    share = remote(core_sums, core_sums, ts_send, ts_recv, sibling)
    share.start()
    q_copy.wait()
    share.wait()

    def slot_rank(dim):
        s = iota((128, 128), dim)
        core = s // 64
        a = lax.rem(s // 8, 8)
        b = lax.rem(s, 8)
        return block_rank(core, a, b)

    before = (slot_rank(1) < slot_rank(0)).astype(f32).astype(bf16)
    all_sums = sums_of[...].reshape(128, 128)
    offset = None
    for piece in three(all_sums):
        part_of = dot(before, piece.astype(bf16))
        offset = part_of if offset is None else offset + part_of
    for h in range(4):
        table[h] = jnp.broadcast_to(offset[:, h : h + 1], (128, 128))

    def tile(part, core, a, b, count, masked):
        keys = count * BLOCK

        def joined(lo, hi):
            return jnp.concatenate([buf[core, a, b + u, lo:hi, :] for u in range(count)], axis=1)

        k_t = joined(0, HEAD)
        right_side = jnp.concatenate(
            [k_t, k_t, joined(HALF, ROWS), jnp.zeros((112, keys), bf16)], axis=0
        )
        scores = dot(q_aug[part], right_side)
        allowed = None
        if masked:
            q_at = part * HALF + lax.rem(iota((4 * HALF, BLOCK), 0), HALF)
            allowed = iota((4 * HALF, BLOCK), 1) <= q_at
            scores = jnp.where(allowed, scores, LOW)
        shifts = []
        highest = None
        for u in range(count):
            slot = core * 64 + a * 8 + b + u
            shift = jnp.concatenate(
                [jnp.broadcast_to(table[h, pl.ds(slot, 1), :], (HALF, 128)) for h in range(4)],
                axis=0,
            )
            s = scores[:, u * BLOCK : (u + 1) * BLOCK]
            most = jnp.maximum(s[:, 0:128], s[:, 128:256]) + shift
            highest = most if highest is None else jnp.maximum(highest, most)
            shifts.append(shift)
        old = peak[part]
        new = jnp.maximum(old, jnp.max(highest, axis=1, keepdims=True))
        weights = []
        for u in range(count):
            base = new - shifts[u]
            for v in range(2):
                at = u * BLOCK + v * 128
                w = jnp.exp2(scores[:, at : at + 128] - base)
                if masked:
                    w = jnp.where(allowed[:, v * 128 : (v + 1) * 128], w, 0.0)
                weights.append(w.astype(bf16))
        v_t = jnp.concatenate(
            [joined(HEAD, HALF), jnp.ones((16, keys), bf16), jnp.zeros((48, keys), bf16)], axis=0
        )
        gained = dot_t(jnp.concatenate(weights, axis=1), v_t)
        accum[part] = accum[part] * jnp.exp2(old - new) + gained
        peak[part] = new

    def process(core, a, ch):
        def one_part(part, carry):
            mine = rank * (1 - part) + (127 - rank) * part
            b = ch * 4
            ranks = [block_rank(core, a, b + u) for u in range(4)]
            full = sum((r < mine).astype(jnp.int32) for r in ranks)
            equal = sum((r == mine).astype(jnp.int32) for r in ranks)

            @pl.when(full == 4)
            def _():
                tile(part, core, a, b, 4, False)

            @pl.when((full == 2) | (full == 3))
            def _():
                tile(part, core, a, b, 2, False)

            @pl.when((full == 1) | (full == 3))
            def _():
                tile(part, core, a, b + full - 1, 1, False)

            @pl.when(equal == 1)
            def _():
                tile(part, core, a, b + full, 1, True)

            return carry

        lax.fori_loop(0, 2, one_part, 0)

    def w_share(k):
        ref = w_all.at[lax.rem(x + 3 - k, 4), half_rows]
        return remote(ref, ref, ws_send.at[k], ws_recv.at[k], sibling)

    def step(t, carry):
        i = t // 4 - 1
        sel = lax.rem(t, 4)
        d = (i + 2) // 2
        side = lax.rem(sel, 2)
        ch = (lax.rem(i + 2, 2) + (i // 6) * side) * jnp.minimum(i + 1, 1) + side * (
            1 - jnp.minimum(i + 1, 1)
        )

        @pl.when((sel == 0) & (i >= 0))
        def _():
            to_right(0, 0, i).wait_recv()

            @pl.when(i <= 4)
            def _():
                to_right(d, ch, i + 2).start()

            to_sibling(lax.rem(a0 - d + 8, 8), ch, 2 + 2 * i).start()

        @pl.when((sel == 1) & (i >= 0))
        def _():
            to_left(0, 0, i).wait_recv()

            @pl.when(i <= 3)
            def _():
                to_left(d, ch, i + 2).start()

            @pl.when(i == 5)
            def _():
                to_left(d, ch, 6).start()

            to_sibling(lax.rem(a0 + d, 8), ch, 3 + 2 * i).start()

        @pl.when(sel >= 2)
        def _():
            to_sibling(a0, 0, 2 * i + sel).wait_recv()

        @pl.when(t == 20)
        def _():
            for k in range(3):
                w_copies[k].wait()
                w_share(k).start()

        core = c * (1 - sel // 2) + (1 - c) * (sel // 2)
        center = a0 * (1 - sel // 2) + b0 * (sel // 2)
        a = lax.rem(center + 8 + d * (2 * side - 1), 8)
        process(core, a, ch)
        return carry

    lax.fori_loop(0, 32, step, 0)

    for part in range(2):
        total_of = accum[part]
        result = total_of[:, 0:HEAD] / total_of[:, HEAD : HEAD + 1]
        for h in range(4):
            att[part, :, h * HEAD : (h + 1) * HEAD] = result[h * HALF : (h + 1) * HALF].astype(bf16)

    def drain(i, carry):
        to_sibling(a0, 0, i).wait_send()
        return carry

    lax.fori_loop(0, 16, drain, 0)

    def drain_ring(i, carry):
        to_right(0, 0, i).wait_send()
        to_left(0, 0, i).wait_send()
        return carry

    lax.fori_loop(0, 7, drain_ring, 0)

    def to(owner):
        part = owner // 2
        device = mirrors[owner] if part else (z, y, c, owner)
        src = att.at[part, pl.ds((owner % 2) * 64, 64), :]
        return remote(src, heads.at[x], att_send.at[owner], att_recv.at[x], device)

    for owner in (2, 3):
        to(owner).start()
    for owner in range(2):

        @pl.when(x != owner)
        def _(owner=owner):
            to(owner).start()

        @pl.when(x == owner)
        def _(owner=owner):
            heads[owner] = att[0, owner * 64 : (owner + 1) * 64, :]

    for k in range(3):
        w_share(k).wait()
    for g in range(4):

        @pl.when((x >= 2) | (x != g))
        def _(g=g):
            src = att.at[0, pl.ds(0, 64), :]
            remote(src, heads.at[g], att_send.at[0], att_recv.at[g], mirrors[0]).wait_recv()

    for col in range(0, out.shape[1], 512):
        total = None
        for g in range(4):
            part = dot(heads[g], w_all[g, :, col : col + 512]).astype(bf16).astype(f32)
            total = part if total is None else total + part
        out[:, col : col + 512] = total.astype(bf16)

    for owner in range(4):
        if owner < 2:

            @pl.when(x != owner)
            def _(owner=owner):
                to(owner).wait_send()
        else:
            to(owner).wait_send()


def shards(tokens, w_query, w_key, w_value, w_gate, gate_bias, w_output):
    d = tokens.shape[1]
    hbm = pl.BlockSpec(memory_space=pltpu.HBM)
    dma = pltpu.SemaphoreType.DMA
    vmem = pltpu.VMEM
    return pl.pallas_call(
        layer_kernel,
        name="layer",
        out_shape=jax.ShapeDtypeStruct(tokens.shape, bf16),
        in_specs=[hbm] * 7,
        out_specs=pl.BlockSpec(memory_space=pltpu.VMEM),
        scratch_shapes=[
            vmem((4, *tokens.shape), bf16),
            vmem(w_query.shape, bf16),
            vmem((HEAD, d), bf16),
            vmem((HEAD, d), bf16),
            vmem((4, d), bf16),
            vmem((1, 4), f32),
            vmem((4, *w_output.shape), bf16),
            vmem((2, 8, 8, ROWS, BLOCK), bf16),
            vmem((2, 8, 8, 1, 128), f32),
            vmem((2, 4 * HALF, 256), bf16),
            vmem((4 * HALF, 128), bf16),
            vmem((2, 4 * HALF, 128), f32),
            vmem((2, 4 * HALF, 128), f32),
            vmem((4, 128, 128), f32),
            vmem((2, HALF, 4 * HEAD), bf16),
            vmem((4, 64, 4 * HEAD), bf16),
            dma((7,)),
            dma((3,)), dma((3,)),
            dma((7,)), dma((7,)),
            dma((7,)), dma((7,)),
            dma((7,)), dma((7,)),
            dma, dma,
            dma((7,)), dma((7,)),
            dma((7,)), dma((7,)),
            dma((16,)), dma((16,)),
            dma, dma,
            dma((3,)), dma((3,)),
            dma((3,)), dma((3,)),
            dma((4,)), dma((4,)),
        ],
        compiler_params=pltpu.CompilerParams(
            collective_id=0, has_side_effects=True, vmem_limit_bytes=56 * 2**20
        ),
    )(tokens, w_query, w_key.T, w_value.T, w_gate.T, gate_bias.reshape(1, -1), w_output)


def solution(mesh):
    finer = Mesh(mesh.devices.reshape(8, 8, 2, mesh.shape["tp"]), AXES)
    placed = (
        P(SP_TP, None),
        P(None, "tp"),
        P(None, "tp"),
        P(None, "tp"),
        P(None, "tp"),
        P("tp"),
        P("tp", None),
    )
    return jax.shard_map(
        shards, mesh=finer, in_specs=placed, out_specs=P(SP_TP, None), check_vma=False
    )
```

time: 390 us -> 99.5 us (0.26)
  the two profiles are of different devices: /device:TPU:504 before, /device:TPU:71 now
where the time goes in v2:
time: 99.5 us; the launch traced here: 99.3 us
  Pallas kernels  97.6 us (98%)
  local copies, waits for them, and re-layouts  1.67 us (2%)
    pallas_call x1, Pallas kernels, shards(): pl.pallas_call(layer_kernel, name='layer', out_shape=jax.ShapeDtypeStruct...  97.6 us

profile of v2, /device:TPU:71, one launch (start us, length us, event | category | flops | bytes accessed | tf_op | source)
XLA Modules:
  0.0 99.3 jit_solution(16713790574171347653)
XLA Ops:
  0.0 97.6 %layer.1 = bf16[64,2048]{1,0:T(8,128)(2,1)} custom-call(bf16[64,2048]{1,0:T(8,128)(2,1)} %tokens.1, bf16[2048,256]{1,0:T(8,128)(2,1)} %w_q.1, bf16[64,2048]{1,0:T(8,128)(2,1)} %bitcast.4, bf16[64,2048]{1,0:T(8,128)(2,1)} %bitcast.5, bf16[4,2048]{1,0:T(4,128)(2,1)} %bitcast.6, f32[1,4]{1,0:T(1,128)} %bitcast.7, bf16[256,2048]{1,0:T(8,128)(2,1)} %w_o.1), custom_call_target="tpu_custom_call" | custom-call | tf_op jit(solution)/shard_map/layer/pallas_call | solution.py:408
  97.6 1.7 %copy.9 = bf16[64,2048]{1,0:T(8,128)(2,1)} copy(bf16[64,2048]{1,0:T(8,128)(2,1)} %layer.1) | data formatting | bytes 524288

commit v3 on v2

--- a/solution.py
+++ b/solution.py
@@ -53,7 +53,7 @@
 
 def layer_kernel(
     tokens, w_q, w_kt, w_vt, w_gt, bias, w_o, out,
-    x_all, wq_v, wk_v, wv_v, wg_v, bias_v, w_all, buf, sums_of, q_aug, q_far, peak, accum, table,
+    x_all, wq_v, wk_v, wv_v, wg_v, bias_v, w_all, buf, sums_of, q_aug, q_far, q_near, peak, accum, table,
     att, heads,
     local, tok_send, tok_recv, one_send, one_recv, ta_send, ta_recv, tb_send, tb_recv,
     ts_send, ts_recv, right_send, right_recv, left_send, left_recv, sib_send, sib_recv,
@@ -62,14 +62,16 @@
     z, y, c, x = (lax.axis_index(a) for a in AXES)
     a0 = z * (1 - c) + y * c
     b0 = y * (1 - c) + z * c
+    my_slot = c * 64 + a0 * 8 + b0
     rank = z * 16 + y * 2 + c
     across = [(z, y, c, lax.rem(x + k, 4)) for k in range(1, 4)]
     ring = [(lax.rem(z + k * c, 8), lax.rem(y + k * (1 - c), 8), c, x) for k in range(1, 8)]
     cross = [(lax.rem(z + k * (1 - c), 8), lax.rem(y + k * c, 8), c, x) for k in range(1, 8)]
     right, left = cross[0], cross[6]
     sibling = (z, y, 1 - c, x)
-    mirrors = [(7 - z, 7 - y, 1 - c, g) for g in range(4)]
-    mirror = (7 - z, 7 - y, 1 - c, x)
+    mirrors = [(7 - z, y, 1 - c, g) for g in range(4)]
+    mirror = (7 - z, y, 1 - c, x)
+    far_rank = (7 - z) * 16 + y * 2 + 1 - c
 
     loads = [
         pltpu.make_async_copy(src, dst, local.at[i])
@@ -87,10 +89,22 @@
     loads[0].wait()
     pl.semaphore_wait(barrier, len(peers))
 
-    toks = [remote(x_all.at[x], x_all.at[x], tok_send.at[k], tok_recv.at[k], across[k]) for k in range(3)]
-    for k in (0, 2, 1):
-        toks[k].start()
-
+    def piece(owner, half):
+        return x_all.at[owner, pl.ds(half * 32, 32)]
+
+    def tok(i):
+        half = (0, 1, 1, 0, 0, 1)[i]
+        owner = (x, x, x, x, lax.rem(x + 3, 4), lax.rem(x + 1, 4))[i]
+        ref = piece(owner, half)
+        return remote(ref, ref, tok_send.at[i], tok_recv.at[i], across[(0, 0, 2, 2, 0, 2)[i]])
+
+    for i in (0, 2, 1, 3):
+        tok(i).start()
+
+    for i in (0, 2):
+        tok(i).wait_recv()
+        tok(4 + i // 2).start()
+    buf[128] = jnp.zeros((ROWS, BLOCK), bf16)
     lanes = iota((4 * HALF, 128), 1)
     selector = (
         (lanes < 12) & (lax.rem(lanes, 4) == iota((4 * HALF, 128), 0) // HALF)
@@ -101,16 +115,16 @@
     accum[...] = jnp.zeros(accum.shape, f32)
     for load in loads[1:]:
         load.wait()
-    for k in range(3):
-        toks[k].wait_recv()
+    for i in (1, 3, 4, 5):
+        tok(i).wait_recv()
 
     rows = x_all[...].reshape(BLOCK, x_all.shape[2])
     gates = dot_t(wg_v[...], rows).astype(bf16).astype(f32)
     spread = jnp.broadcast_to(bias_v[...], (4, 4))
     column = jnp.sum(jnp.where(iota((4, 4), 0) == iota((4, 4), 1), spread, 0.0), axis=1, keepdims=True)
     gates = jnp.concatenate([gates + column, jnp.zeros((4, BLOCK), f32)], axis=0)
-    buf[c, a0, b0, 0:HEAD, :] = dot_t(wk_v[...], rows).astype(bf16)
-    buf[c, a0, b0, HEAD:HALF, :] = dot_t(wv_v[...], rows).astype(bf16)
+    buf[my_slot, 0:HEAD, :] = dot_t(wk_v[...], rows).astype(bf16)
+    buf[my_slot, HEAD:HALF, :] = dot_t(wv_v[...], rows).astype(bf16)
     small = jnp.exp(-jnp.abs(gates))
     series = small * (1.0 - small * (0.5 - small * (1 / 3 - small * (0.25 - small * 0.2))))
     logs = jnp.minimum(gates, 0.0) - jnp.where(small < 0.02, series, jnp.log(1.0 + small))
@@ -125,28 +139,33 @@
     last = jnp.broadcast_to(decay[:, BLOCK - 1 : BLOCK], (8, 128))
     ends = jnp.where((iota((8, 128), 0) == iota((8, 128), 1)) & (iota((8, 128), 0) < 4), last, 0.0)
     sums_of[c, a0, b0] = jnp.sum(ends, axis=0, keepdims=True)
-    buf[c, a0, b0, HALF:ROWS, :] = jnp.concatenate([first, second], axis=0).astype(bf16)
+    buf[my_slot, HALF:ROWS, :] = jnp.concatenate([first, second], axis=0).astype(bf16)
 
     own_sum = sums_of.at[c, a0, b0]
     tas = [remote(own_sum, own_sum, ta_send.at[k], ta_recv.at[k], ring[k]) for k in range(7)]
     for k in range(7):
         tas[k].start()
-    own = buf.at[c, a0, b0]
+    own = buf.at[my_slot]
     ones = [remote(own, own, one_send.at[k], one_recv.at[k], ring[k]) for k in range(7)]
-    for k in (0, 6, 1, 5, 2, 4, 3):
+    for k in (3, 2, 4, 1, 5, 0, 6):
         ones[k].start()
 
-    queries = dot(rows, wq_v[...]).astype(bf16).astype(f32) * (LOG2E * HEAD**-0.5)
-    top = queries.astype(bf16).astype(f32)
-    rest = queries - top
-    for h in range(4):
-        cols = slice(h * HEAD, (h + 1) * HEAD)
-        both = jnp.concatenate([top[:, cols], rest[:, cols]], axis=1).astype(bf16)
-        q_aug[0, h * HALF : (h + 1) * HALF, 0:128] = both[0:HALF]
-        q_far[h * HALF : (h + 1) * HALF, :] = both[HALF:]
-    for k in range(3):
-        toks[k].wait_send()
-    q_copy = remote(q_far, q_aug.at[1, :, pl.ds(0, 128)], q_send, q_recv, mirror)
+    queries = dot(rows, wq_v[...]).astype(bf16)
+    q_far[...] = queries[HALF:]
+
+    def expand(part, raw):
+        scaled = raw.astype(f32) * (LOG2E * HEAD**-0.5)
+        top = scaled.astype(bf16).astype(f32)
+        rest = scaled - top
+        for h in range(4):
+            cols = slice(h * HEAD, (h + 1) * HEAD)
+            both = jnp.concatenate([top[:, cols], rest[:, cols]], axis=1)
+            q_aug[part, h * HALF : (h + 1) * HALF, 0:128] = both.astype(bf16)
+
+    expand(0, queries[0:HALF])
+    for i in range(6):
+        tok(i).wait_send()
+    q_copy = remote(q_far, q_near, q_send, q_recv, mirror)
     q_copy.start()
     half_rows = pl.ds(pl.multiple_of(c * 128, 128), 128)
     own_half = w_all.at[x, half_rows]
@@ -162,7 +181,7 @@
         tbs[k].start()
 
     def chunk(core, a, ch):
-        return buf.at[core, a, pl.ds(ch * 4, 4)]
+        return buf.at[pl.ds(core * 64 + a * 8 + ch * 4, 4)]
 
     def to_right(d, ch, i):
         ref = chunk(c, lax.rem(a0 - d + 8, 8), ch)
@@ -180,7 +199,7 @@
         ones[k].wait()
     for ch in range(2):
         to_right(0, ch, ch).start()
-        to_left(0, ch, ch).start()
+        to_left(0, 1 - ch, ch).start()
     for ch in range(2):
         to_sibling(a0, ch, ch).start()
 
@@ -190,6 +209,7 @@
     share = remote(core_sums, core_sums, ts_send, ts_recv, sibling)
     share.start()
     q_copy.wait()
+    expand(1, q_near[...])
     share.wait()
 
     def slot_rank(dim):
@@ -206,13 +226,15 @@
         part_of = dot(before, piece.astype(bf16))
         offset = part_of if offset is None else offset + part_of
     for h in range(4):
-        table[h] = jnp.broadcast_to(offset[:, h : h + 1], (128, 128))
-
-    def tile(part, core, a, b, count, masked):
+        table[h, 0:128] = jnp.broadcast_to(offset[:, h : h + 1], (128, 128))
+        table[h, 128:136] = jnp.full((8, 128), LOW, f32)
+
+    def tile(part, slots, masked):
+        count = len(slots)
         keys = count * BLOCK
 
         def joined(lo, hi):
-            return jnp.concatenate([buf[core, a, b + u, lo:hi, :] for u in range(count)], axis=1)
+            return jnp.concatenate([buf[slot, lo:hi, :] for slot in slots], axis=1)
 
         k_t = joined(0, HEAD)
         right_side = jnp.concatenate(
@@ -227,9 +249,8 @@
         shifts = []
         highest = None
         for u in range(count):
-            slot = core * 64 + a * 8 + b + u
             shift = jnp.concatenate(
-                [jnp.broadcast_to(table[h, pl.ds(slot, 1), :], (HALF, 128)) for h in range(4)],
+                [jnp.broadcast_to(table[h, pl.ds(slots[u], 1), :], (HALF, 128)) for h in range(4)],
                 axis=0,
             )
             s = scores[:, u * BLOCK : (u + 1) * BLOCK]
@@ -254,88 +275,119 @@
         accum[part] = accum[part] * jnp.exp2(old - new) + gained
         peak[part] = new
 
-    def process(core, a, ch):
-        def one_part(part, carry):
-            mine = rank * (1 - part) + (127 - rank) * part
-            b = ch * 4
-            ranks = [block_rank(core, a, b + u) for u in range(4)]
-            full = sum((r < mine).astype(jnp.int32) for r in ranks)
-            equal = sum((r == mine).astype(jnp.int32) for r in ranks)
-
-            @pl.when(full == 4)
-            def _():
-                tile(part, core, a, b, 4, False)
-
-            @pl.when((full == 2) | (full == 3))
-            def _():
-                tile(part, core, a, b, 2, False)
-
-            @pl.when((full == 1) | (full == 3))
-            def _():
-                tile(part, core, a, b + full - 1, 1, False)
-
-            @pl.when(equal == 1)
-            def _():
-                tile(part, core, a, b + full, 1, True)
-
-            return carry
-
-        lax.fori_loop(0, 2, one_part, 0)
-
     def w_share(k):
         ref = w_all.at[lax.rem(x + 3 - k, 4), half_rows]
         return remote(ref, ref, ws_send.at[k], ws_recv.at[k], sibling)
 
-    def step(t, carry):
-        i = t // 4 - 1
-        sel = lax.rem(t, 4)
+    def arrival(i, side, core):
         d = (i + 2) // 2
-        side = lax.rem(sel, 2)
-        ch = (lax.rem(i + 2, 2) + (i // 6) * side) * jnp.minimum(i + 1, 1) + side * (
-            1 - jnp.minimum(i + 1, 1)
-        )
-
-        @pl.when((sel == 0) & (i >= 0))
+        later = jnp.minimum(i + 1, 1)
+        odd = lax.rem(i + 2, 2)
+        ch = (odd * (1 - side) + (1 - odd) * side) * later + side * (1 - later)
+        center = z * (1 - core) + y * core
+        return lax.rem(center + 8 + d * (2 * side - 1), 8), ch
+
+    owners = (rank, far_rank)
+    diagonals = (
+        my_slot,
+        (1 - c) * 64 + ((7 - z) * c + y * (1 - c)) * 8 + y * c + (7 - z) * (1 - c),
+    )
+
+    def needed(n):
+        starts = []
+        numbers = ([], [])
+        for i, core, live in ((n - 1, c, n <= 7), (n - 2, 1 - c, n >= 1)):
+            at = jnp.maximum(jnp.minimum(i, 6), -1)
+            for side in range(2):
+                a, ch = arrival(at, side, core)
+                starts.append(core * 64 + a * 8 + ch * 4)
+                for part in range(2):
+                    whole = sum(
+                        (block_rank(core, a, ch * 4 + u) < owners[part]).astype(jnp.int32)
+                        for u in range(4)
+                    )
+                    numbers[part].append(whole * live.astype(jnp.int32))
+        return starts, numbers
+
+    def pick(k, starts, number):
+        first, second = number[0], number[0] + number[1]
+        third = second + number[2]
+        fourth = third + number[3]
+        slot = jnp.where(k < third, starts[2] + k - second, starts[3] + k - third)
+        slot = jnp.where(k < second, starts[1] + k - first, slot)
+        slot = jnp.where(k < first, starts[0] + k, slot)
+        return jnp.where(k < fourth, slot, 128)
+
+    def round_of(n, kept):
+        i = n - 1
+
+        @pl.when((n >= 1) & (n <= 7))
         def _():
+            d = (i + 2) // 2
+            a_r, ch_r = arrival(i, 0, c)
+            a_l, ch_l = arrival(i, 1, c)
             to_right(0, 0, i).wait_recv()
 
             @pl.when(i <= 4)
             def _():
-                to_right(d, ch, i + 2).start()
-
-            to_sibling(lax.rem(a0 - d + 8, 8), ch, 2 + 2 * i).start()
-
-        @pl.when((sel == 1) & (i >= 0))
+                to_right(d, ch_r, i + 2).start()
+
+            to_left(0, 0, i).wait_recv()
+
+            @pl.when(i <= 4)
+            def _():
+                to_left(d, ch_l, i + 2).start()
+
+            to_sibling(a_r, ch_r, 2 + 2 * i).start()
+            to_sibling(a_l, ch_l, 3 + 2 * i).start()
+
+        @pl.when(n >= 1)
         def _():
-            to_left(0, 0, i).wait_recv()
-
-            @pl.when(i <= 3)
-            def _():
-                to_left(d, ch, i + 2).start()
-
-            @pl.when(i == 5)
-            def _():
-                to_left(d, ch, 6).start()
-
-            to_sibling(lax.rem(a0 + d, 8), ch, 3 + 2 * i).start()
-
-        @pl.when(sel >= 2)
-        def _():
-            to_sibling(a0, 0, 2 * i + sel).wait_recv()
-
-        @pl.when(t == 20)
+            to_sibling(a0, 0, 2 * i).wait_recv()
+            to_sibling(a0, 0, 2 * i + 1).wait_recv()
+
+        @pl.when(n == 6)
         def _():
             for k in range(3):
                 w_copies[k].wait()
                 w_share(k).start()
 
-        core = c * (1 - sel // 2) + (1 - c) * (sel // 2)
-        center = a0 * (1 - sel // 2) + b0 * (sel // 2)
-        a = lax.rem(center + 8 + d * (2 * side - 1), 8)
-        process(core, a, ch)
-        return carry
-
-    lax.fori_loop(0, 32, step, 0)
+        @pl.when((n == 0) | (n == 7))
+        def _():
+            part = n // 7
+            tile(part, [diagonals[0] * (1 - part) + diagonals[1] * part], True)
+
+        starts, numbers = needed(n)
+        fresh = [sum(numbers[part]) for part in range(2)]
+        tiles = [(kept[part][0] + fresh[part] + 7 * (n // 8)) // 8 for part in range(2)]
+
+        def one_tile(k, carry):
+            part = (k >= tiles[0]).astype(jnp.int32)
+            first = (k - part * tiles[0]) * 8
+            number = [numbers[0][q] * (1 - part) + numbers[1][q] * part for q in range(4)]
+            held = [kept[0][q] * (1 - part) + kept[1][q] * part for q in range(8)]
+            slots = []
+            for u in range(8):
+                slot = pick(first + u - held[0], starts, number)
+                if u < 7:
+                    slot = jnp.where(first + u < held[0], held[1 + u], slot)
+                slots.append(slot)
+            tile(part, slots, False)
+            return carry
+
+        lax.fori_loop(0, tiles[0] + tiles[1], one_tile, 0)
+        after = []
+        for part in range(2):
+            first = tiles[part] * 8
+            rest = [jnp.maximum(kept[part][0] + fresh[part] - first, 0)]
+            for u in range(7):
+                slot = pick(first + u - kept[part][0], starts, numbers[part])
+                rest.append(jnp.where(first + u < kept[part][0], kept[part][1 + u], slot))
+            after.append(tuple(rest))
+        return tuple(after)
+
+    nothing = tuple(jnp.int32(0) for _ in range(8))
+    lax.fori_loop(0, 9, round_of, (nothing, nothing))
 
     for part in range(2):
         total_of = accum[part]
@@ -419,17 +471,18 @@
             vmem((4, d), bf16),
             vmem((1, 4), f32),
             vmem((4, *w_output.shape), bf16),
-            vmem((2, 8, 8, ROWS, BLOCK), bf16),
+            vmem((129, ROWS, BLOCK), bf16),
             vmem((2, 8, 8, 1, 128), f32),
             vmem((2, 4 * HALF, 256), bf16),
-            vmem((4 * HALF, 128), bf16),
+            vmem((HALF, 4 * HEAD), bf16),
+            vmem((HALF, 4 * HEAD), bf16),
             vmem((2, 4 * HALF, 128), f32),
             vmem((2, 4 * HALF, 128), f32),
-            vmem((4, 128, 128), f32),
+            vmem((4, 136, 128), f32),
             vmem((2, HALF, 4 * HEAD), bf16),
             vmem((4, 64, 4 * HEAD), bf16),
             dma((7,)),
-            dma((3,)), dma((3,)),
+            dma((6,)), dma((6,)),
             dma((7,)), dma((7,)),
             dma((7,)), dma((7,)),
             dma((7,)), dma((7,)),

time: 99.5 us -> 80.6 us (0.81)
  the two profiles are of different devices: /device:TPU:71 before, /device:TPU:55 now
where the time goes in v3:
time: 80.6 us; the launch traced here: 80.5 us
  Pallas kernels  78.8 us (98%)
  local copies, waits for them, and re-layouts  1.67 us (2%)
    pallas_call x1, Pallas kernels, shards(): pl.pallas_call(layer_kernel, name='layer', out_shape=jax.ShapeDtypeStruct...  78.8 us
    unnamed x1, local copies, waits for them, and re-layouts  1.67 us

profile of v3, /device:TPU:55, one launch (start us, length us, event | category | flops | bytes accessed | tf_op | source)
XLA Modules:
  0.0 80.5 jit_solution(9711314924529711855)
XLA Ops:
  0.0 78.8 %layer.1 = bf16[64,2048]{1,0:T(8,128)(2,1)} custom-call(bf16[64,2048]{1,0:T(8,128)(2,1)} %tokens.1, bf16[2048,256]{1,0:T(8,128)(2,1)} %w_q.1, bf16[64,2048]{1,0:T(8,128)(2,1)} %bitcast.4, bf16[64,2048]{1,0:T(8,128)(2,1)} %bitcast.5, bf16[4,2048]{1,0:T(4,128)(2,1)} %bitcast.6, f32[1,4]{1,0:T(1,128)} %bitcast.7, bf16[256,2048]{1,0:T(8,128)(2,1)} %w_o.1), custom_call_target="tpu_custom_call" | custom-call | tf_op jit(solution)/shard_map/layer/pallas_call | solution.py:460
  78.8 1.7 %copy.9 = bf16[64,2048]{1,0:T(8,128)(2,1)} copy(bf16[64,2048]{1,0:T(8,128)(2,1)} %layer.1) | data formatting | bytes 524288

commit v4 on v3

--- a/solution.py
+++ b/solution.py
@@ -318,6 +318,31 @@
         slot = jnp.where(k < first, starts[0] + k, slot)
         return jnp.where(k < fourth, slot, 128)
 
+    def to(owner):
+        part = owner // 2
+        device = mirrors[owner] if part else (z, y, c, owner)
+        src = att.at[part, pl.ds((owner % 2) * 64, 64), :]
+        return remote(src, heads.at[x], att_send.at[owner], att_recv.at[x], device)
+
+    def finish(part):
+        total_of = accum[part]
+        result = total_of[:, 0:HEAD] / total_of[:, HEAD : HEAD + 1]
+        for h in range(4):
+            att[part, :, h * HEAD : (h + 1) * HEAD] = result[h * HALF : (h + 1) * HALF].astype(bf16)
+        if part:
+            to(2).start()
+            to(3).start()
+            return
+        for owner in range(2):
+
+            @pl.when(x != owner)
+            def _(owner=owner):
+                to(owner).start()
+
+            @pl.when(x == owner)
+            def _(owner=owner):
+                heads[owner] = att[0, owner * 64 : (owner + 1) * 64, :]
+
     def round_of(n, kept):
         i = n - 1
 
@@ -362,8 +387,8 @@
         tiles = [(kept[part][0] + fresh[part] + 7 * (n // 8)) // 8 for part in range(2)]
 
         def one_tile(k, carry):
-            part = (k >= tiles[0]).astype(jnp.int32)
-            first = (k - part * tiles[0]) * 8
+            part = (k < tiles[1]).astype(jnp.int32)
+            first = (k - (1 - part) * tiles[1]) * 8
             number = [numbers[0][q] * (1 - part) + numbers[1][q] * part for q in range(4)]
             held = [kept[0][q] * (1 - part) + kept[1][q] * part for q in range(8)]
             slots = []
@@ -373,7 +398,16 @@
                     slot = jnp.where(first + u < held[0], held[1 + u], slot)
                 slots.append(slot)
             tile(part, slots, False)
+
+            @pl.when((n == 8) & (k == tiles[1] - 1))
+            def _():
+                finish(1)
+
             return carry
+
+        @pl.when((n == 8) & (tiles[1] == 0))
+        def _():
+            finish(1)
 
         lax.fori_loop(0, tiles[0] + tiles[1], one_tile, 0)
         after = []
@@ -389,12 +423,10 @@
     nothing = tuple(jnp.int32(0) for _ in range(8))
     lax.fori_loop(0, 9, round_of, (nothing, nothing))
 
-    for part in range(2):
-        total_of = accum[part]
-        result = total_of[:, 0:HEAD] / total_of[:, HEAD : HEAD + 1]
-        for h in range(4):
-            att[part, :, h * HEAD : (h + 1) * HEAD] = result[h * HALF : (h + 1) * HALF].astype(bf16)
-
+    finish(0)
+
+    for k in range(3):
+        w_share(k).wait()
     def drain(i, carry):
         to_sibling(a0, 0, i).wait_send()
         return carry
@@ -408,26 +440,6 @@
 
     lax.fori_loop(0, 7, drain_ring, 0)
 
-    def to(owner):
-        part = owner // 2
-        device = mirrors[owner] if part else (z, y, c, owner)
-        src = att.at[part, pl.ds((owner % 2) * 64, 64), :]
-        return remote(src, heads.at[x], att_send.at[owner], att_recv.at[x], device)
-
-    for owner in (2, 3):
-        to(owner).start()
-    for owner in range(2):
-
-        @pl.when(x != owner)
-        def _(owner=owner):
-            to(owner).start()
-
-        @pl.when(x == owner)
-        def _(owner=owner):
-            heads[owner] = att[0, owner * 64 : (owner + 1) * 64, :]
-
-    for k in range(3):
-        w_share(k).wait()
     for g in range(4):
 
         @pl.when((x >= 2) | (x != g))

time: 80.6 us -> 79.2 us (0.983)
  the two profiles are of different devices: /device:TPU:55 before, /device:TPU:64 now
where the time goes in v4:
time: 79.2 us; the launch traced here: 79 us
  Pallas kernels  77.4 us (98%)
  local copies, waits for them, and re-layouts  1.67 us (2%)
    pallas_call x1, Pallas kernels, shards(): pl.pallas_call(layer_kernel, name='layer', out_shape=jax.ShapeDtypeStruct...  77.4 us
    unnamed x1, local copies, waits for them, and re-layouts  1.67 us

profile of v4, /device:TPU:64, one launch (start us, length us, event | category | flops | bytes accessed | tf_op | source)
XLA Modules:
  0.0 79.0 jit_solution(15821480388438442749)
XLA Ops:
  0.0 77.4 %layer.1 = bf16[64,2048]{1,0:T(8,128)(2,1)} custom-call(bf16[64,2048]{1,0:T(8,128)(2,1)} %tokens.1, bf16[2048,256]{1,0:T(8,128)(2,1)} %w_q.1, bf16[64,2048]{1,0:T(8,128)(2,1)} %bitcast.4, bf16[64,2048]{1,0:T(8,128)(2,1)} %bitcast.5, bf16[4,2048]{1,0:T(4,128)(2,1)} %bitcast.6, f32[1,4]{1,0:T(1,128)} %bitcast.7, bf16[256,2048]{1,0:T(8,128)(2,1)} %w_o.1), custom_call_target="tpu_custom_call" | custom-call | tf_op jit(solution)/shard_map/layer/pallas_call | solution.py:472
  77.4 1.7 %copy.9 = bf16[64,2048]{1,0:T(8,128)(2,1)} copy(bf16[64,2048]{1,0:T(8,128)(2,1)} %layer.1) | data formatting | bytes 524288
